TPU v7x, 32 devices: a whole 2x2x4 slice. The times are simulated.
32 devices in a mesh: kv: 8 (over z, x), tp: 4 (over y, core).
Axes of the slice: x: 2, y: 2, z: 4, core: 2. Of those that a mesh axis runs over, the one named last changes fastest.
Arguments:
- tokens: bfloat16 [16384, 2048], P('kv'), may hold values from -6 to 6
- norm_gain: bfloat16 [2048], replicated, may hold values from 0.099609375 to 1.8984375
- query_weight: bfloat16 [2048, 1024], P(None, 'tp'), may hold values from -0.125 to 0.125
- cmp_key_weight: bfloat16 [2048, 512], P(None, 'tp'), may hold values from -0.125 to 0.125
- cmp_value_weight: bfloat16 [2048, 512], P(None, 'tp'), may hold values from -0.125 to 0.125
- sel_key_weight: bfloat16 [2048, 512], P(None, 'tp'), may hold values from -0.125 to 0.125
- sel_value_weight: bfloat16 [2048, 512], P(None, 'tp'), may hold values from -0.125 to 0.125
- branch_weight: bfloat16 [2, 2048, 16], replicated, may hold values from -0.125 to 0.125
- key_embed: bfloat16 [8, 32, 64], P('tp'), may hold values from -3 to 3
- key_inner: bfloat16 [8, 2048, 64], P('tp'), may hold values from -0.125 to 0.125
- key_outer: bfloat16 [8, 64, 64], P('tp'), may hold values from -0.75 to 0.75
- value_embed: bfloat16 [8, 32, 64], P('tp'), may hold values from -3 to 3
- value_inner: bfloat16 [8, 2048, 64], P('tp'), may hold values from -0.125 to 0.125
- value_outer: bfloat16 [8, 64, 64], P('tp'), may hold values from -0.75 to 0.75
- out_weight: bfloat16 [1024, 2048], replicated, may hold values from -0.1875 to 0.1875
- chosen: int32 [8, 128, 8], P('tp'), may hold values from 0 to 255, as said below
Outputs:
- attended: bfloat16 [16384, 2048], P(('kv', 'tp'))
Inputs may be any that keep to these rules, and one draw needn't show every extreme that they name: `chosen`: each entry is the index of a block of 64 positions in the whole sequence. For every key head and query block, its 8 entries lie in 8 different aligned spans of 2048 positions (at most one from any span), and none lies inside the query block's own positions.
All inputs are finite; a program needn't handle non-finite values.
Results may differ from a plain program's by a relative error of at most 0.0075.
Values may be sent and summed in bfloat16 or wider, within the bound.
A program may use at most 128 MiB of HBM per device.

v0:
```python
import functools

import jax
import jax.numpy as jnp
from jax import lax
from jax.experimental import pallas as pl
from jax.experimental.pallas import tpu as pltpu
from jax.sharding import PartitionSpec as P

HEAD_DIM = 64
CMP_BLOCK = 32
SEL_BLOCK = 64
Q_BLOCK = 128
FAR_PICKS = 8
LANES = 2 * HEAD_DIM
PLANES = 4
MESH = pl.DeviceIdType.MESH

ROPE_BASE = 10000.0
norm_eps = 1e-06
MASKED = -1e30

def params(n_axes, limit=48):
    return pltpu.CompilerParams(
        dimension_semantics=("arbitrary",) * n_axes, vmem_limit_bytes=limit * 1024 * 1024
    )


def norm_rows(tok_ref, gain_ref):
    x = tok_ref[...].astype(jnp.float32)
    inv = lax.rsqrt(jnp.mean(x * x, axis=-1, keepdims=True) + norm_eps)
    return (x * inv * gain_ref[...].astype(jnp.float32)).astype(jnp.bfloat16)


def turn(x, cosine, sine_up, sine_down):
    quarter = HEAD_DIM // 2
    return (
        x * cosine
        + pltpu.roll(x, LANES - quarter, 1) * sine_up
        + pltpu.roll(x, quarter, 1) * sine_down
    )


def low_lanes(shape):
    return lax.broadcasted_iota(jnp.int32, shape, 1) < HEAD_DIM


def sel_kernel(tok_ref, gain_ref, w_ref, cos_ref, up_ref, down_ref, *outs):
    normed = norm_rows(tok_ref, gain_ref)
    y = jnp.dot(normed, w_ref[...], preferred_element_type=jnp.float32)
    for k, out in enumerate(outs):
        x = y[:, k * LANES : (k + 1) * LANES]
        low = low_lanes(x.shape)
        turned = turn(x, cos_ref[...], up_ref[...], down_ref[...])
        out[...] = jnp.where(low, turned, x).astype(jnp.bfloat16)


def nt_dot(a, b):
    return lax.dot_general(a, b, (((1,), (1,)), ((), ())), preferred_element_type=jnp.float32)


def gate_lanes(gate, first, shape):
    return jnp.where(low_lanes(shape), gate[:, first : first + 1], gate[:, first + 1 : first + 2])


def merge(out, rows):
    low = low_lanes((rows, LANES))
    return jnp.where(low, pltpu.roll(out[:rows], HEAD_DIM, 1), out[rows:])


def exchange_kernel(
    planes,
    idx_ref,
    bias_ref,
    gain_ref,
    ke_ref,
    ko_ref,
    ve_ref,
    vo_ref,
    tok_hbm,
    w_hbm,
    cos_hbm,
    up_hbm,
    down_hbm,
    ki_hbm,
    vi_hbm,
    *rest,
):
    kv_local = bias_ref.shape[0]
    own_hbm, rest = rest[:kv_local], rest[kv_local:]
    out_ref, rest = rest[0], rest[1:]
    held, rest = rest[:kv_local], rest[kv_local:]
    (
        tok,
        w,
        cosine,
        up,
        down,
        ki,
        vi,
        qp,
        qt,
        ck,
        cv,
        gate,
        sums,
        oc,
        mix,
        got,
        local_sem,
        send_sem,
        recv_sem,
        sum_send,
        sum_recv,
        mix_send,
        mix_recv,
    ) = rest
    owners, ranks = sums.shape[0], got.shape[0]
    rows, width = tok.shape
    span = rows // SEL_BLOCK
    across = owners // planes
    me, rank = lax.axis_index("kv"), lax.axis_index("tp")
    z, x = me // across, me % across

    barrier = pltpu.get_barrier_semaphore()
    for d in range(1, owners):
        pl.semaphore_signal(barrier, inc=1, device_id={"kv": (me + d) % owners}, device_id_type=MESH)
    for d in range(1, ranks):
        pl.semaphore_signal(barrier, inc=1, device_id={"tp": (rank + d) % ranks}, device_id_type=MESH)
    loads = [
        (tok_hbm, tok),
        (w_hbm, w),
        (cos_hbm, cosine),
        (up_hbm, up),
        (down_hbm, down),
        (ki_hbm, ki),
        (vi_hbm, vi),
    ]
    copies = [pltpu.make_async_copy(a, b, local_sem.at[n]) for n, (a, b) in enumerate(loads)]
    for k in range(kv_local):
        copies.append(
            pltpu.make_async_copy(own_hbm[k], held[k].at[pl.ds(0, span)], local_sem.at[len(loads) + k])
        )
    for copy in copies:
        copy.start()
    pl.semaphore_wait(barrier, owners + ranks - 2)

    def slot(k, n):
        return held[k].at[pl.ds(n * span, span)]

    def hop(k, dz, dx):
        n = dz * across + dx
        if dx:
            source = own_hbm[k] if dz == 0 else slot(k, dz * across)
            target = z * across + (x + dx) % across
            sends = (x + dx < across) if dz == 0 else (z >= dz)
            gets = (x >= dx) if dz == 0 else (z >= dz)
        else:
            step = 1 if dz == 3 else dz
            source = slot(k, 2 * across) if dz == 3 else own_hbm[k]
            target = lax.rem(me + step * across, owners)
            sends = (z == 2) if dz == 3 else (z + dz < planes)
            gets = z >= dz
        copy = pltpu.make_async_remote_copy(
            src_ref=source,
            dst_ref=slot(k, n),
            send_sem=send_sem.at[k, n],
            recv_sem=recv_sem.at[k, n],
            device_id={"kv": target},
            device_id_type=MESH,
        )
        return copy, sends, gets

    def send(k, dz, dx):
        copy, sends, _ = hop(k, dz, dx)
        pl.when(sends)(copy.start)

    def arrive(k, dz, dx):
        copy, _, gets = hop(k, dz, dx)
        pl.when(gets)(copy.wait_recv)

    def send_own(k):
        for dz in (2, 1):
            if dz < planes:
                send(k, dz, 0)
        for dx in range(1, across):
            send(k, 0, dx)

    def forward(k, dz):
        if dz >= planes:
            return
        arrive(k, dz, 0)
        if dz == 2 and planes > 3:
            send(k, 3, 0)
        for dx in range(1, across):
            send(k, dz, dx)

    send_own(0)
    for copy in copies:
        copy.wait()

    tile = 256
    scale = HEAD_DIM ** (-0.5)
    base = kv_local * LANES
    kv_width = kv_local * HEAD_DIM

    def project(i, carry):
        at = pl.ds(pl.multiple_of(i * tile, tile), tile)
        normed = norm_rows(tok.at[at], gain_ref)
        y = jnp.dot(normed, w[...], preferred_element_type=jnp.float32)
        for k in range(kv_local):
            v = y[:, k * LANES : (k + 1) * LANES]
            low = low_lanes(v.shape)
            turned = turn(v, cosine[at], up[at], down[at]) * scale
            for ref, q in ((qp, v * scale), (qt, turned)):
                ref[k, 0, at] = jnp.where(low, q, 0.0).astype(jnp.bfloat16)
                ref[k, 1, at] = jnp.where(low, pltpu.roll(q, HEAD_DIM, 1), 0.0).astype(jnp.bfloat16)
        ck[at] = y[:, base : base + kv_width].astype(jnp.bfloat16).astype(jnp.float32)
        cv[at] = y[:, base + kv_width : base + 2 * kv_width].astype(jnp.bfloat16).astype(jnp.float32)
        gate[at] = jax.nn.sigmoid(y[:, base + 2 * kv_width :])
        return carry

    lax.fori_loop(0, rows // tile, project, 0)

    blocks = rows // CMP_BLOCK

    def summarize(x_ref, e_ref, i_ref, o_ref):
        parts = []
        for c in range(CMP_BLOCK):
            part = x_ref[pl.ds(c, blocks, stride=CMP_BLOCK), :] + e_ref[c : c + 1, :]
            parts.append(part.astype(jnp.bfloat16))
        flat = jnp.concatenate(parts, axis=1)
        hidden = jnp.dot(flat, i_ref[...], preferred_element_type=jnp.float32)
        hidden = jax.nn.gelu(hidden).astype(jnp.bfloat16)
        return jnp.dot(hidden, o_ref[...], preferred_element_type=jnp.float32)

    sk = summarize(ck, ke_ref, ki, ko_ref)
    sv = summarize(cv, ve_ref, vi, vo_ref)
    for k in range(kv_local):
        cut = slice(k * HEAD_DIM, (k + 1) * HEAD_DIM)
        sums[me, k] = jnp.concatenate([sk[:, cut], sv[:, cut]], axis=1).astype(jnp.bfloat16)

    def sum_copy(d, source):
        return pltpu.make_async_remote_copy(
            src_ref=sums.at[source],
            dst_ref=sums.at[source],
            send_sem=sum_send.at[d],
            recv_sem=sum_recv.at[d],
            device_id={"kv": (me + d) % owners},
            device_id_type=MESH,
        )

    for d in range(1, owners):
        sum_copy(d, me).start()
    for k in range(1, kv_local):
        send_own(k)
    forward(0, 2)
    forward(0, 1)
    for d in range(1, owners):
        sum_copy(d, (me + owners - d) % owners).wait_recv()

    def compress(i, carry):
        at = pl.ds(pl.multiple_of(i * tile, tile), tile)
        row = lax.broadcasted_iota(jnp.int32, (2 * tile, 1), 0)
        pos = me * rows + i * tile + jnp.where(row >= tile, row - tile, row)
        lane = lax.broadcasted_iota(jnp.int32, (1, owners * blocks), 1)
        allowed = (lane + 1) * CMP_BLOCK - 1 <= pos
        for k in range(kv_local):
            keys = jnp.concatenate([sums[s, k] for s in range(owners)], axis=0)
            q = jnp.concatenate([qp[k, 0, at], qp[k, 1, at]], axis=0)
            s = jnp.where(allowed, nt_dot(q, keys), MASKED)
            top = jnp.max(s, axis=-1, keepdims=True)
            e = jnp.where(allowed, jnp.exp(s - top), 0.0)
            total = jnp.sum(e, axis=-1, keepdims=True)
            o = jnp.dot(e.astype(jnp.bfloat16), keys, preferred_element_type=jnp.float32)
            o = o * jnp.where(total > 0.0, 1.0 / jnp.where(total > 0.0, total, 1.0), 0.0)
            o = merge(o, tile)
            oc[k, at] = o * gate_lanes(gate[at], 2 * k, o.shape)
        return carry

    lax.fori_loop(0, rows // tile, compress, 0)

    rank_rows = rows // ranks
    group = rank_rows // Q_BLOCK
    q_blocks = rows // Q_BLOCK
    half_gates = 2 * kv_local

    def mix_copy(k, step):
        target = (rank + 1 + step) % ranks
        at = pl.ds(pl.multiple_of(target * rank_rows, rank_rows), rank_rows)
        return pltpu.make_async_remote_copy(
            src_ref=mix.at[k, at],
            dst_ref=got.at[rank, k],
            send_sem=mix_send.at[k, step],
            recv_sem=mix_recv.at[k, step],
            device_id={"tp": target},
            device_id_type=MESH,
        )

    def choose(k):
        def one(step, carry):
            target = (rank + 1 + step) % ranks
            for u in range(group):
                j = target * group + u
                at = pl.ds(pl.multiple_of(j * Q_BLOCK, Q_BLOCK), Q_BLOCK)
                own = j * (Q_BLOCK // SEL_BLOCK)
                parts = [held[k][own + b] for b in range(Q_BLOCK // SEL_BLOCK)]
                for a in range(FAR_PICKS):
                    pick = idx_ref[(k * q_blocks + j) * FAR_PICKS + a]
                    parts.append(held[k][pick])
                keys = jnp.concatenate(parts, axis=0)
                q = jnp.concatenate([qt[k, 0, at], qt[k, 1, at]], axis=0)
                s = nt_dot(q, keys) + bias_ref[k, j]
                row = lax.broadcasted_iota(jnp.int32, (2 * Q_BLOCK, Q_BLOCK), 0)
                row = jnp.where(row >= Q_BLOCK, row - Q_BLOCK, row)
                lane = lax.broadcasted_iota(jnp.int32, row.shape, 1)
                near = jnp.where(lane > row, MASKED, s[:, :Q_BLOCK])
                s = jnp.concatenate([near, s[:, Q_BLOCK:]], axis=1)
                top = jnp.max(s, axis=-1, keepdims=True)
                e = jnp.exp(s - top)
                total = jnp.sum(e, axis=-1, keepdims=True)
                o = jnp.dot(e.astype(jnp.bfloat16), keys, preferred_element_type=jnp.float32)
                o = merge(o * (1.0 / total), Q_BLOCK)
                g = gate_lanes(gate[at], half_gates + 2 * k, o.shape)
                mix[k, at] = (oc[k, at] + o * g).astype(jnp.bfloat16)
            pl.when(step > 0)(lambda: mix_copy(k, step - 1).start())
            return carry

        lax.fori_loop(0, ranks, one, 0)

    moves = [(dz, dx) for dz in range(planes) for dx in range(across) if (dz, dx) != (0, 0)]
    for k in range(kv_local):
        if k:
            forward(k, 2)
            forward(k, 1)
        forward(k, 3)
        for dz, dx in moves:
            if dx:
                arrive(k, dz, dx)
        choose(k)
    own_at = pl.ds(pl.multiple_of(rank * rank_rows, rank_rows), rank_rows)
    for k in range(kv_local):
        for dz, dx in moves:
            copy, sends, _ = hop(k, dz, dx)
            pl.when(sends)(copy.wait_send)
    for d in range(1, owners):
        sum_copy(d, me).wait_send()
    for k in range(kv_local):
        got[rank, k] = mix[k, own_at]
        for step in range(ranks - 1):
            mix_copy(k, step).wait_send()
            mix_copy(k, step).wait_recv()
    for t in range(ranks):
        for k in range(kv_local):
            first = (t * kv_local + k) * LANES
            out_ref[:, first : first + LANES] = got[t, k]


def cost(flops, moved):
    return pl.CostEstimate(flops=int(flops), bytes_accessed=int(moved), transcendentals=0)


def block_diagonal(w):
    n, a, b = w.shape
    zero = jnp.zeros((a, b), w.dtype)
    return jnp.concatenate(
        [jnp.concatenate([w[i] if i == j else zero for j in range(n)], axis=1) for i in range(n)],
        axis=0,
    )


def inner_diagonal(w):
    n, rows, e = w.shape
    w = w.reshape(n, CMP_BLOCK, HEAD_DIM, e)
    zero = jnp.zeros_like(w[0])
    full = jnp.stack(
        [jnp.concatenate([w[i] if i == j else zero for j in range(n)], axis=-1) for i in range(n)],
        axis=1,
    )
    return full.reshape(CMP_BLOCK * n * HEAD_DIM, n * e)


def per_device(
    tokens,
    norm_gain,
    query_weight,
    cmp_key_weight,
    cmp_value_weight,
    sel_key_weight,
    sel_value_weight,
    branch_weight,
    key_embed,
    key_inner,
    key_outer,
    value_embed,
    value_inner,
    value_outer,
    out_weight,
    chosen,
):
    rows, width = tokens.shape
    kv_local = key_embed.shape[0]
    heads_local = query_weight.shape[1] // HEAD_DIM
    owners = lax.axis_size("kv")
    me = lax.axis_index("kv")
    planes = PLANES if owners % PLANES == 0 else 1
    across = owners // planes
    my_z, my_x = me // across, me % across
    offset = me * rows
    f32 = jnp.float32
    bf16 = jnp.bfloat16

    half = HEAD_DIM // 2
    lane = jnp.arange(LANES, dtype=jnp.int32)
    inverse = ROPE_BASE ** (-(lane % half).astype(f32) / half)
    positions = offset + jnp.arange(rows, dtype=jnp.int32)
    phases = positions.astype(f32)[:, None] * inverse[None, :]
    cosine = jnp.cos(phases)
    sine = jnp.sin(phases)
    first = (lane % HEAD_DIM < half)[None, :]
    up = jnp.where(first, -sine, 0.0)
    down = jnp.where(first, 0.0, sine)
    gain = norm_gain.reshape(1, width)

    def heads_of(w, k):
        return w[:, k * HEAD_DIM : (k + 1) * HEAD_DIM]

    sel_weight = jnp.concatenate(
        [heads_of(w, k) for k in range(kv_local) for w in (sel_key_weight, sel_value_weight)],
        axis=1,
    )
    tile = 256
    steps = rows // tile
    row_spec = lambda cols: pl.BlockSpec((tile, cols), lambda i: (i, 0))
    full = lambda shape: pl.BlockSpec(shape, lambda *_: (0,) * len(shape))
    kv = pl.pallas_call(
        sel_kernel,
        grid=(steps,),
        in_specs=[row_spec(width), full((1, width)), full(sel_weight.shape)]
        + [row_spec(LANES)] * 3,
        out_specs=[row_spec(LANES)] * kv_local,
        out_shape=[jax.ShapeDtypeStruct((rows, LANES), bf16)] * kv_local,
        compiler_params=params(1),
        cost_estimate=cost(2 * rows * width * sel_weight.shape[1], rows * width * 2),
        name="sel_project",
    )(tokens, gain, sel_weight, cosine, up, down)

    gate_cols = lax.dynamic_slice_in_dim(
        branch_weight, lax.axis_index("tp") * heads_local, heads_local, 2
    )
    gate_weight = jnp.concatenate([gate_cols[0], gate_cols[1]], axis=1)
    gate_count = 2 * heads_local
    mid_weight = jnp.concatenate(
        [query_weight, cmp_key_weight, cmp_value_weight, jnp.pad(gate_weight, ((0, 0), (0, LANES - gate_count)))],
        axis=1,
    )
    kv_width = kv_local * HEAD_DIM
    blocks = rows // CMP_BLOCK
    embeds = [
        e.astype(f32).transpose(1, 0, 2).reshape(CMP_BLOCK, kv_width)
        for e in (key_embed, value_embed)
    ]
    q_blocks = rows // Q_BLOCK
    span_blocks = rows // SEL_BLOCK
    picks = lax.dynamic_slice_in_dim(chosen.astype(jnp.int32), me * q_blocks, q_blocks, 1)
    own_first = (me * q_blocks + jnp.arange(q_blocks, dtype=jnp.int32)) * (Q_BLOCK // SEL_BLOCK)
    usable = picks < own_first[None, :, None]
    span = picks // span_blocks
    slot = (my_z - span // across) * across + (my_x - span % across) % across
    index = jnp.where(usable, slot * span_blocks + picks % span_blocks, 0).reshape(-1)
    bias = jnp.where(usable, 0.0, MASKED).astype(f32)
    bias = jnp.repeat(bias, SEL_BLOCK, axis=-1)
    bias = jnp.pad(bias, ((0, 0), (0, 0), (Q_BLOCK, 0)))[:, :, None, :]

    ranks = lax.axis_size("tp")
    rank_rows = rows // ranks
    key_diag, value_diag = inner_diagonal(key_inner), inner_diagonal(value_inner)
    operands = (
        index,
        bias,
        gain,
        embeds[0],
        block_diagonal(key_outer),
        embeds[1],
        block_diagonal(value_outer),
        tokens,
        mid_weight,
        cosine,
        up,
        down,
        key_diag,
        value_diag,
        *[own.reshape(span_blocks, SEL_BLOCK, LANES) for own in kv],
    )
    vmem = pl.BlockSpec(memory_space=pltpu.VMEM)
    hbm = pl.BlockSpec(memory_space=pl.ANY)
    dma = pltpu.SemaphoreType.DMA
    spread = pltpu.VMEM((kv_local, 2, rows, LANES), bf16)
    gathered = pl.pallas_call(
        functools.partial(exchange_kernel, planes),
        in_specs=[pl.BlockSpec(memory_space=pltpu.SMEM)] + [vmem] * 6 + [hbm] * (7 + kv_local),
        out_specs=vmem,
        out_shape=jax.ShapeDtypeStruct((rank_rows, ranks * kv_local * LANES), bf16),
        scratch_shapes=[pltpu.VMEM((owners * span_blocks, SEL_BLOCK, LANES), bf16)] * kv_local
        + [
            pltpu.VMEM(tokens.shape, bf16),
            pltpu.VMEM(mid_weight.shape, bf16),
            pltpu.VMEM(cosine.shape, f32),
            pltpu.VMEM(cosine.shape, f32),
            pltpu.VMEM(cosine.shape, f32),
            pltpu.VMEM(key_diag.shape, bf16),
            pltpu.VMEM(value_diag.shape, bf16),
            spread,
            spread,
            pltpu.VMEM((rows, kv_width), f32),
            pltpu.VMEM((rows, kv_width), f32),
            pltpu.VMEM((rows, LANES), f32),
            pltpu.VMEM((owners, kv_local, blocks, LANES), bf16),
            pltpu.VMEM((kv_local, rows, LANES), f32),
            pltpu.VMEM((kv_local, rows, LANES), bf16),
            pltpu.VMEM((ranks, kv_local, rank_rows, LANES), bf16),
            dma((7 + kv_local,)),
            dma((kv_local, owners)),
            dma((kv_local, owners)),
            dma((owners,)),
            dma((owners,)),
            dma((kv_local, ranks)),
            dma((kv_local, ranks)),
        ],
        compiler_params=pltpu.CompilerParams(
            collective_id=0, has_side_effects=True, vmem_limit_bytes=60 * 1024 * 1024
        ),
        cost_estimate=cost(4e10, 2e7),
        name="exchange",
    )(*operands)
    return jnp.dot(gathered, out_weight, preferred_element_type=f32).astype(bf16)


def solution(mesh):
    placed = (
        P("kv", None),
        P(),
        P(None, "tp"),
        P(None, "tp"),
        P(None, "tp"),
        P(None, "tp"),
        P(None, "tp"),
        P(),
        P("tp", None, None),
        P("tp", None, None),
        P("tp", None, None),
        P("tp", None, None),
        P("tp", None, None),
        P("tp", None, None),
        P(),
        P("tp", None, None),
    )
    return jax.shard_map(
        per_device, mesh=mesh, in_specs=placed, out_specs=P(("kv", "tp"), None), check_vma=False
    )
```

profile of v0, /device:TPU:27, one launch (start us, length us, event | category | flops | bytes accessed | tf_op | source)
XLA Modules:
  0.0 172.4 jit_solution(8510922876027208964)
XLA Ops:
  0.0 0.8 broadcast_select_fusion
  0.8 0.8 fusion.16
  1.6 0.7 reshape.74.idx_ref
  2.3 2.0 %fusion.27 = (bf16[2048,64]{1,0:T(8,128)(2,1)S(1)}, bf16[2048,64]{1,0:T(8,128)(2,1)S(1)}, bf16[2048,64]{1,0:T(8,128)(2,1)S(1)}, bf16[2048,64]{1,0:T(8,128)(2,1)S(1)}) fusion(bf16[2048,128]{1,0:T(8,128)(2,1)} %param.21, bf16[2048,128]{1,0:T(8,128)(2,1)} %param.22), kind=kLoop, calls=%fused_computation.70 | loop fusion | bytes 2097152 | tf_op jit(solution)/shard_map/slice | solution.py:426
  4.3 0.7 pad_maximum_fusion.2.w_ref
  5.1 3.8 %fusion.2 = (f32[2048,128]{1,0:T(8,128)S(1)}, f32[2048,128]{1,0:T(8,128)S(1)}, f32[2048,128]{1,0:T(8,128)S(1)}) fusion(f32[128]{0:T(128)S(1)} %fusion.25, f32[2048]{0:T(1024)S(1)} %add_convert_fusion, pred[128]{0:T(512)(128)(4,1)S(1)} %fusion.26), kind=kLoop, calls=%fused_computation.6 | loop fusion | flops 1048576 | bytes 3154560 | tf_op jit(solution)/shard_map/jit(_where)/select_n | solution.py:422
  9.0 10.9 %sel_project.1 = (bf16[2048,128]{1,0:T(8,128)(2,1)S(1)}, bf16[2048,128]{1,0:T(8,128)(2,1)S(1)}) custom-call(bf16[2048,2048]{1,0:T(8,128)(2,1)} %tok_hbm.1, bf16[1,2048]{1,0:T(2,128)(2,1)S(1)} %reshape.76.gain_ref, bf16[2048,256]{1,0:T(8,128)(2,1)S(1)} %pad_maximum_fusion.2.w_ref, f32[2048,128]{1,0:T(8,128)S(1)} %get-tuple-element.27.cos_ref.cos_hbm, ...), custom_call_target="tpu_custom_call" | custom-call | flops 2147483648 | bytes 8388608 | tf_op jit(solution)/shard_map/sel_project/pallas_call | solution.py:436
  19.9 0.8 copy-done.4
  20.8 0.9 copy-done.5
  21.9 0.7 broadcast_in_dim.45.bias_ref
  22.6 0.8 dynamic-slice_bitcast_fusion.1
  23.7 1.7 fusion.1.w_hbm
  25.4 0.3 copy.44
  25.7 0.3 copy.43
  26.0 0.3 pad_bitcast_fusion.2
  26.3 1.1 pad_maximum_fusion
  27.5 0.3 copy.45
  28.1 0.3 pad_bitcast_fusion
  28.4 1.1 pad_maximum_fusion.1
  29.5 0.7 fusion.9
  30.3 0.7 reshape.86.ke_ref
  31.0 0.7 reshape.88.ve_ref
  31.7 134.5 %exchange.1 = bf16[512,1024]{1,0:T(8,128)(2,1)} custom-call(s32[256]{0:T(256)} %reshape.74.idx_ref, f32[2,16,1,640]{3,2,1,0:T(1,128)} %broadcast_in_dim.45.bias_ref, bf16[1,2048]{1,0:T(2,128)(2,1)} %copy-done.3, f32[32,128]{1,0:T(8,128)} %reshape.86.ke_ref, bf16[128,128]{1,0:T(8,128)(2,1)} %get-tuple-element.34.ko_ref, f32[32,128]{1,0:T(8,128)} %reshape.88.ve_ref, ...), custom_call_target="tpu_custom_call" | custom-call | flops 40000000000 | bytes 20000000 | tf_op jit(solution)/shard_map/exchange/pallas_call | solution.py:499
  166.2 6.2 %convolution_convert_fusion = bf16[512,2048]{1,0:T(8,128)(2,1)} fusion(bf16[512,1024]{1,0:T(8,128)(2,1)} %exchange.1, bf16[1024,2048]{1,0:T(8,128)(2,1)} %param.30), kind=kOutput, calls=%fused_computation.2 | convolution fusion | flops 2148532224 | bytes 7340032 | tf_op jit(solution)/shard_map/dot_general | solution.py:536
  (51 shorter events, 1.2 us)
Async XLA Ops:
  4.3 4.6 %copy-start.15 = (bf16[2048]{0:T(1024)(128)(2,1)S(1)}, bf16[2048]{0:T(1024)(128)(2,1)}, u32[]{:S(2)}) copy-start(bf16[2048]{0:T(1024)(128)(2,1)} %param.17) | copy-start | bytes 12292
  8.9 11.0 %copy-start = (f32[2048,128]{1,0:T(8,128)}, f32[2048,128]{1,0:T(8,128)S(1)}, u32[]{:S(2)}) copy-start(f32[2048,128]{1,0:T(8,128)S(1)} %get-tuple-element.25.down_ref.down_hbm) | copy-start | bytes 3145732
  8.9 11.0 %copy-start.1 = (f32[2048,128]{1,0:T(8,128)}, f32[2048,128]{1,0:T(8,128)S(1)}, u32[]{:S(2)}) copy-start(f32[2048,128]{1,0:T(8,128)S(1)} %get-tuple-element.26.up_ref.up_hbm) | copy-start | bytes 3145732
  8.9 11.0 %copy-start.2 = (f32[2048,128]{1,0:T(8,128)}, f32[2048,128]{1,0:T(8,128)S(1)}, u32[]{:S(2)}) copy-start(f32[2048,128]{1,0:T(8,128)S(1)} %get-tuple-element.27.cos_ref.cos_hbm) | copy-start | bytes 3145732
  9.0 10.9 %copy-start.3 = (bf16[1,2048]{1,0:T(2,128)(2,1)}, bf16[1,2048]{1,0:T(2,128)(2,1)S(1)}, u32[]{:S(2)}) copy-start(bf16[1,2048]{1,0:T(2,128)(2,1)S(1)} %reshape.76.gain_ref) | copy-start | bytes 12292
  9.0 14.7 %copy-start.6 = (bf16[2048,256]{1,0:T(8,128)(2,1)S(1)}, bf16[2048,256]{1,0:T(8,128)(2,1)}, u32[]{:S(2)}) copy-start(bf16[2048,256]{1,0:T(8,128)(2,1)} %param.18) | copy-start | bytes 3145732
  9.0 14.7 %copy-start.7 = (bf16[2048,128]{1,0:T(8,128)(2,1)S(1)}, bf16[2048,128]{1,0:T(8,128)(2,1)}, u32[]{:S(2)}) copy-start(bf16[2048,128]{1,0:T(8,128)(2,1)} %param.20) | copy-start | bytes 1572868
  9.0 14.7 %copy-start.8 = (bf16[2048,128]{1,0:T(8,128)(2,1)S(1)}, bf16[2048,128]{1,0:T(8,128)(2,1)}, u32[]{:S(2)}) copy-start(bf16[2048,128]{1,0:T(8,128)(2,1)} %param.19) | copy-start | bytes 1572868
  19.9 0.9 copy-start.4
  20.8 0.9 copy-start.5
  23.7 1.7 copy-start.9
  25.7 1.7 copy-start.10
  27.8 1.7 %copy-start.11 = (bf16[2,64,64]{2,1,0:T(8,128)(2,1)S(1)}, bf16[2,64,64]{2,1,0:T(8,128)(2,1)}, u32[]{:S(2)}) copy-start(bf16[2,64,64]{2,1,0:T(8,128)(2,1)} %param.29) | copy-start | bytes 49156
  27.8 1.7 %copy-start.12 = (bf16[2,64,64]{2,1,0:T(8,128)(2,1)S(1)}, bf16[2,64,64]{2,1,0:T(8,128)(2,1)}, u32[]{:S(2)}) copy-start(bf16[2,64,64]{2,1,0:T(8,128)(2,1)} %param.26) | copy-start | bytes 49156
  27.8 2.4 %copy-start.13 = (bf16[2,32,64]{2,1,0:T(8,128)(2,1)S(1)}, bf16[2,32,64]{2,1,0:T(8,128)(2,1)}, u32[]{:S(2)}) copy-start(bf16[2,32,64]{2,1,0:T(8,128)(2,1)} %param.24) | copy-start | bytes 24580
  27.8 3.2 %copy-start.14 = (bf16[2,32,64]{2,1,0:T(8,128)(2,1)S(1)}, bf16[2,32,64]{2,1,0:T(8,128)(2,1)}, u32[]{:S(2)}) copy-start(bf16[2,32,64]{2,1,0:T(8,128)(2,1)} %param.27) | copy-start | bytes 24580
where the time goes:
time: 173 us; the launch traced here: 172 us
  Pallas kernels  145 us (84%)
  other arithmetic  10.7 us (6%)
  local copies, waits for them, and re-layouts  9.79 us (6%)
  matrix products  6.17 us (4%)
    pallas_call x1, Pallas kernels, per_device(): pl.pallas_call(functools.partial(exchange_kernel, planes), in_specs=[pl.B...  134 us
    pallas_call x1, Pallas kernels, per_device(): pl.pallas_call(sel_kernel, grid=(steps,), in_specs=[row_spec(width), full...  10.9 us
    dot_general x1, matrix products, per_device(): jnp.dot(gathered, out_weight, preferred_element_type=f32).astype(bf16)  6.17 us
    select_n x1, other arithmetic, per_device(): down = jnp.where(first, 0.0, sine)  3.79 us

commit v1 on v0

--- a/solution.py
+++ b/solution.py
@@ -156,10 +156,9 @@
             sends = (x + dx < across) if dz == 0 else (z >= dz)
             gets = (x >= dx) if dz == 0 else (z >= dz)
         else:
-            step = 1 if dz == 3 else dz
-            source = slot(k, 2 * across) if dz == 3 else own_hbm[k]
-            target = lax.rem(me + step * across, owners)
-            sends = (z == 2) if dz == 3 else (z + dz < planes)
+            source = slot(k, (dz - 1) * across) if dz > 1 else own_hbm[k]
+            target = lax.rem(me + across, owners)
+            sends = (z >= dz - 1) & (z + 1 < planes)
             gets = z >= dz
         copy = pltpu.make_async_remote_copy(
             src_ref=source,
@@ -180,9 +179,8 @@
         pl.when(gets)(copy.wait_recv)
 
     def send_own(k):
-        for dz in (2, 1):
-            if dz < planes:
-                send(k, dz, 0)
+        if planes > 1:
+            send(k, 1, 0)
         for dx in range(1, across):
             send(k, 0, dx)
 
@@ -190,12 +188,13 @@
         if dz >= planes:
             return
         arrive(k, dz, 0)
-        if dz == 2 and planes > 3:
-            send(k, 3, 0)
+        if dz + 1 < planes:
+            send(k, dz + 1, 0)
         for dx in range(1, across):
             send(k, dz, dx)
 
-    send_own(0)
+    for k in range(kv_local):
+        send_own(k)
     for copy in copies:
         copy.wait()
 
@@ -225,14 +224,15 @@
     blocks = rows // CMP_BLOCK
 
     def summarize(x_ref, e_ref, i_ref, o_ref):
+        embed = jnp.concatenate([e_ref[k].astype(jnp.float32) for k in range(kv_local)], axis=1)
         parts = []
         for c in range(CMP_BLOCK):
-            part = x_ref[pl.ds(c, blocks, stride=CMP_BLOCK), :] + e_ref[c : c + 1, :]
+            part = x_ref[pl.ds(c, blocks, stride=CMP_BLOCK), :] + embed[c : c + 1]
             parts.append(part.astype(jnp.bfloat16))
         flat = jnp.concatenate(parts, axis=1)
-        hidden = jnp.dot(flat, i_ref[...], preferred_element_type=jnp.float32)
+        hidden = jnp.dot(flat, inner_diagonal(i_ref[...]), preferred_element_type=jnp.float32)
         hidden = jax.nn.gelu(hidden).astype(jnp.bfloat16)
-        return jnp.dot(hidden, o_ref[...], preferred_element_type=jnp.float32)
+        return jnp.dot(hidden, block_diagonal(o_ref[...]), preferred_element_type=jnp.float32)
 
     sk = summarize(ck, ke_ref, ki, ko_ref)
     sv = summarize(cv, ve_ref, vi, vo_ref)
@@ -252,10 +252,8 @@
 
     for d in range(1, owners):
         sum_copy(d, me).start()
-    for k in range(1, kv_local):
-        send_own(k)
-    forward(0, 2)
-    forward(0, 1)
+    for k in range(kv_local):
+        forward(k, 1)
     for d in range(1, owners):
         sum_copy(d, (me + owners - d) % owners).wait_recv()
 
@@ -278,7 +276,14 @@
             oc[k, at] = o * gate_lanes(gate[at], 2 * k, o.shape)
         return carry
 
-    lax.fori_loop(0, rows // tile, compress, 0)
+    tiles = rows // tile
+    bounds = [tiles * k // kv_local for k in range(kv_local + 1)]
+    for k in range(kv_local):
+        lax.fori_loop(bounds[k], bounds[k + 1], compress, 0)
+        forward(k, 2)
+    for dz in range(3, planes):
+        for k in range(kv_local):
+            forward(k, dz)
 
     rank_rows = rows // ranks
     group = rank_rows // Q_BLOCK
@@ -330,10 +335,6 @@
 
     moves = [(dz, dx) for dz in range(planes) for dx in range(across) if (dz, dx) != (0, 0)]
     for k in range(kv_local):
-        if k:
-            forward(k, 2)
-            forward(k, 1)
-        forward(k, 3)
         for dz, dx in moves:
             if dx:
                 arrive(k, dz, dx)
@@ -370,14 +371,14 @@
 
 
 def inner_diagonal(w):
-    n, rows, e = w.shape
-    w = w.reshape(n, CMP_BLOCK, HEAD_DIM, e)
-    zero = jnp.zeros_like(w[0])
-    full = jnp.stack(
-        [jnp.concatenate([w[i] if i == j else zero for j in range(n)], axis=-1) for i in range(n)],
-        axis=1,
-    )
-    return full.reshape(CMP_BLOCK * n * HEAD_DIM, n * e)
+    n, _, e = w.shape
+    zero = jnp.zeros((HEAD_DIM, e), w.dtype)
+    parts = []
+    for c in range(CMP_BLOCK):
+        for i in range(n):
+            cut = w[i, c * HEAD_DIM : (c + 1) * HEAD_DIM]
+            parts.append(jnp.concatenate([cut if i == j else zero for j in range(n)], axis=1))
+    return jnp.concatenate(parts, axis=0)
 
 
 def per_device(
@@ -456,10 +457,6 @@
     )
     kv_width = kv_local * HEAD_DIM
     blocks = rows // CMP_BLOCK
-    embeds = [
-        e.astype(f32).transpose(1, 0, 2).reshape(CMP_BLOCK, kv_width)
-        for e in (key_embed, value_embed)
-    ]
     q_blocks = rows // Q_BLOCK
     span_blocks = rows // SEL_BLOCK
     picks = lax.dynamic_slice_in_dim(chosen.astype(jnp.int32), me * q_blocks, q_blocks, 1)
@@ -474,22 +471,21 @@
 
     ranks = lax.axis_size("tp")
     rank_rows = rows // ranks
-    key_diag, value_diag = inner_diagonal(key_inner), inner_diagonal(value_inner)
     operands = (
         index,
         bias,
         gain,
-        embeds[0],
-        block_diagonal(key_outer),
-        embeds[1],
-        block_diagonal(value_outer),
+        key_embed,
+        key_outer,
+        value_embed,
+        value_outer,
         tokens,
         mid_weight,
         cosine,
         up,
         down,
-        key_diag,
-        value_diag,
+        key_inner,
+        value_inner,
         *[own.reshape(span_blocks, SEL_BLOCK, LANES) for own in kv],
     )
     vmem = pl.BlockSpec(memory_space=pltpu.VMEM)
@@ -508,8 +504,8 @@
             pltpu.VMEM(cosine.shape, f32),
             pltpu.VMEM(cosine.shape, f32),
             pltpu.VMEM(cosine.shape, f32),
-            pltpu.VMEM(key_diag.shape, bf16),
-            pltpu.VMEM(value_diag.shape, bf16),
+            pltpu.VMEM(key_inner.shape, bf16),
+            pltpu.VMEM(value_inner.shape, bf16),
             spread,
             spread,
             pltpu.VMEM((rows, kv_width), f32),

time: 173 us -> 146 us (0.84)
  Pallas kernels: 145 us -> 121 us
  other arithmetic: 10.7 us -> 7.78 us
    pallas_call x1, Pallas kernels: 134 us -> 110 us  [per_device(): pl.pallas_call(functools.partial(exchange_kernel, planes), in_specs=[pl.B...]
    unnamed x32 -> x24, local copies, waits for them, and re-layouts: 1.79 us -> 5.41 us
    another operation x2 -> x0, other arithmetic: 2.18 us -> none  [inner_diagonal(): jnp.stack([jnp.concatenate([w[i] if i == j else zero for j in range(n)],...]
where the time goes in v1:
time: 146 us
  Pallas kernels  121 us (83%)
  local copies, waits for them, and re-layouts  10.2 us (7%)
  other arithmetic  7.78 us (5%)
  matrix products  6.17 us (4%)
    pallas_call x1, Pallas kernels, per_device(): pl.pallas_call(functools.partial(exchange_kernel, planes), in_specs=[pl.B...  110 us
    pallas_call x1, Pallas kernels, per_device(): pl.pallas_call(sel_kernel, grid=(steps,), in_specs=[row_spec(width), full...  10.8 us
    dot_general x1, matrix products, per_device(): jnp.dot(gathered, out_weight, preferred_element_type=f32).astype(bf16)  6.17 us
    unnamed x24, local copies, waits for them, and re-layouts  5.41 us
    select_n x1, other arithmetic, per_device(): down = jnp.where(first, 0.0, sine)  3.79 us

profile of v1, /device:TPU:27, one launch (start us, length us, event | category | flops | bytes accessed | tf_op | source)
XLA Modules:
  0.0 145.6 jit_solution(4344219773329248390)
XLA Ops:
  0.0 0.8 broadcast_select_fusion
  0.8 0.8 fusion.10
  1.6 0.1 copy.26
  1.6 0.7 reshape.48.idx_ref
  2.3 2.0 %fusion.21 = (bf16[2048,64]{1,0:T(8,128)(2,1)S(1)}, bf16[2048,64]{1,0:T(8,128)(2,1)S(1)}, bf16[2048,64]{1,0:T(8,128)(2,1)S(1)}, bf16[2048,64]{1,0:T(8,128)(2,1)S(1)}) fusion(bf16[2048,128]{1,0:T(8,128)(2,1)} %param.21, bf16[2048,128]{1,0:T(8,128)(2,1)} %param.22), kind=kLoop, calls=%fused_computation.50 | loop fusion | bytes 2097152 | tf_op jit(solution)/shard_map/slice | solution.py:427
  4.3 0.7 pad_maximum_fusion.w_ref
  5.1 3.8 %fusion.2 = (f32[2048,128]{1,0:T(8,128)S(1)}, f32[2048,128]{1,0:T(8,128)S(1)}, f32[2048,128]{1,0:T(8,128)S(1)}) fusion(f32[128]{0:T(128)S(1)} %fusion.19, f32[2048]{0:T(1024)S(1)} %add_convert_fusion, pred[128]{0:T(512)(128)(4,1)S(1)} %fusion.20), kind=kLoop, calls=%fused_computation.6 | loop fusion | flops 1048576 | bytes 3154560 | tf_op jit(solution)/shard_map/jit(_where)/select_n | solution.py:423
  8.9 0.0 copy-start.2
  9.0 0.0 copy-start.7
  9.0 0.0 copy-start.8
  9.0 10.8 %sel_project.1 = (bf16[2048,128]{1,0:T(8,128)(2,1)S(1)}, bf16[2048,128]{1,0:T(8,128)(2,1)S(1)}) custom-call(bf16[2048,2048]{1,0:T(8,128)(2,1)} %tok_hbm.1, bf16[1,2048]{1,0:T(2,128)(2,1)S(1)} %reshape.50.gain_ref, bf16[2048,256]{1,0:T(8,128)(2,1)S(1)} %pad_maximum_fusion.w_ref, f32[2048,128]{1,0:T(8,128)S(1)} %get-tuple-element.19.cos_ref.cos_hbm, ...), custom_call_target="tpu_custom_call" | custom-call | flops 2147483648 | bytes 8388608 | tf_op jit(solution)/shard_map/sel_project/pallas_call | solution.py:437
  19.9 0.8 copy-done.4
  20.7 0.8 copy-done.5
  21.6 0.1 copy.27
  21.6 0.1 broadcast_in_dim.44
  21.7 0.1 reshape.49
  21.9 0.7 broadcast_in_dim.45.bias_ref
  22.5 0.8 dynamic-slice_bitcast_fusion.1
  23.4 0.3 copy.28
  23.7 1.7 %fusion.1.w_hbm = bf16[2048,640]{1,0:T(8,128)(2,1)} fusion(bf16[2048,8]{1,0:T(8,128)(2,1)S(1)} %copy.28, bf16[2048,128]{1,0:T(8,128)(2,1)S(1)} %copy-done.7, bf16[2048,128]{1,0:T(8,128)(2,1)S(1)} %copy-done.8, bf16[2048,256]{1,0:T(8,128)(2,1)S(1)} %copy-done.6), kind=kLoop, calls=%fused_computation.3 | loop fusion | flops 13107200 | bytes 4751360 | tf_op jit(solution)/shard_map/concatenate | solution.py:454
  25.3 1.3 copy.29.ki_hbm
  26.7 2.4 %copy.30.vi_hbm = bf16[2,2048,64]{2,1,0:T(8,128)(2,1)} copy(bf16[2,2048,64]{1,2,0:T(8,128)(2,1)} %param.28) | data formatting | bytes 1048576 | tf_op args[12]
  29.0 110.4 %exchange.1 = bf16[512,1024]{1,0:T(8,128)(2,1)} custom-call(s32[256]{0:T(256)} %reshape.48.idx_ref, f32[2,16,1,640]{3,2,1,0:T(1,128)} %broadcast_in_dim.45.bias_ref, bf16[1,2048]{1,0:T(2,128)(2,1)} %copy-done.3, bf16[2,32,64]{2,1,0:T(8,128)(2,1)} %ke_ref.1, bf16[2,64,64]{2,1,0:T(8,128)(2,1)} %ko_ref.1, bf16[2,32,64]{2,1,0:T(8,128)(2,1)} %ve_ref.1, ...), custom_call_target="tpu_custom_call" | custom-call | flops 40000000000 | bytes 20000000 | tf_op jit(solution)/shard_map/exchange/pallas_call | solution.py:495
  139.5 6.2 %convolution_convert_fusion = bf16[512,2048]{1,0:T(8,128)(2,1)} fusion(bf16[512,1024]{1,0:T(8,128)(2,1)} %exchange.1, bf16[1024,2048]{1,0:T(8,128)(2,1)} %param.30), kind=kOutput, calls=%fused_computation.2 | convolution fusion | flops 2148532224 | bytes 7340032 | tf_op jit(solution)/shard_map/dot_general | solution.py:532
  (24 shorter events, 0.1 us)
Async XLA Ops:
  4.3 4.6 %copy-start.10 = (bf16[2048]{0:T(1024)(128)(2,1)S(1)}, bf16[2048]{0:T(1024)(128)(2,1)}, u32[]{:S(2)}) copy-start(bf16[2048]{0:T(1024)(128)(2,1)} %param.17) | copy-start | bytes 12292
  8.9 11.0 %copy-start = (f32[2048,128]{1,0:T(8,128)}, f32[2048,128]{1,0:T(8,128)S(1)}, u32[]{:S(2)}) copy-start(f32[2048,128]{1,0:T(8,128)S(1)} %get-tuple-element.17.down_ref.down_hbm) | copy-start | bytes 3145732
  8.9 11.0 %copy-start.1 = (f32[2048,128]{1,0:T(8,128)}, f32[2048,128]{1,0:T(8,128)S(1)}, u32[]{:S(2)}) copy-start(f32[2048,128]{1,0:T(8,128)S(1)} %get-tuple-element.18.up_ref.up_hbm) | copy-start | bytes 3145732
  8.9 11.0 %copy-start.2 = (f32[2048,128]{1,0:T(8,128)}, f32[2048,128]{1,0:T(8,128)S(1)}, u32[]{:S(2)}) copy-start(f32[2048,128]{1,0:T(8,128)S(1)} %get-tuple-element.19.cos_ref.cos_hbm) | copy-start | bytes 3145732
  9.0 10.9 %copy-start.3 = (bf16[1,2048]{1,0:T(2,128)(2,1)}, bf16[1,2048]{1,0:T(2,128)(2,1)S(1)}, u32[]{:S(2)}) copy-start(bf16[1,2048]{1,0:T(2,128)(2,1)S(1)} %reshape.50.gain_ref) | copy-start | bytes 12292
  9.0 14.7 %copy-start.6 = (bf16[2048,256]{1,0:T(8,128)(2,1)S(1)}, bf16[2048,256]{1,0:T(8,128)(2,1)}, u32[]{:S(2)}) copy-start(bf16[2048,256]{1,0:T(8,128)(2,1)} %param.18) | copy-start | bytes 3145732
  9.0 14.7 %copy-start.7 = (bf16[2048,128]{1,0:T(8,128)(2,1)S(1)}, bf16[2048,128]{1,0:T(8,128)(2,1)}, u32[]{:S(2)}) copy-start(bf16[2048,128]{1,0:T(8,128)(2,1)} %param.20) | copy-start | bytes 1572868
  9.0 14.7 %copy-start.8 = (bf16[2048,128]{1,0:T(8,128)(2,1)S(1)}, bf16[2048,128]{1,0:T(8,128)(2,1)}, u32[]{:S(2)}) copy-start(bf16[2048,128]{1,0:T(8,128)(2,1)} %param.19) | copy-start | bytes 1572868
  19.9 0.8 copy-start.4
  20.7 0.8 copy-start.5
  23.7 1.7 %copy-start.9 = (bf16[2,2048,64]{1,2,0:T(8,128)(2,1)S(1)}, bf16[2,2048,64]{1,2,0:T(8,128)(2,1)}, u32[]{:S(2)}) copy-start(bf16[2,2048,64]{1,2,0:T(8,128)(2,1)} %param.25) | copy-start | bytes 1572868
